TPU v7x, 32 devices: a whole 2x2x4 slice. The times are simulated.
32 devices in a mesh: fs: 8 (over z, y), tp: 4 (over x, core).
Axes of the slice: x: 2, y: 2, z: 4, core: 2. Of those that a mesh axis runs over, the one named last changes fastest.
Arguments:
- tokens: bfloat16 [6144, 2048], P('fs', 'tp'), may hold values from -40 to 40
- gain_one: float32 [2048], P('tp'), may hold values from 0.1 to 1.9
- w_gate: float32 [2048, 3072], P('fs', 'tp'), may hold values from -0.125 to 0.125
- w_up: float32 [2048, 3072], P('fs', 'tp'), may hold values from -0.125 to 0.125
- w_down: float32 [3072, 2048], P('tp', 'fs'), may hold values from -0.109375 to 0.109375
- scale_gate: float32 [3072], P('tp'), may hold values from 0.5 to 2
- scale_up: float32 [3072], P('tp'), may hold values from 0.5 to 2
- scale_down: float32 [2048], P('tp'), may hold values from 0.5 to 2
- gain_mix: float32 [2048], P('tp'), may hold values from 0.1 to 1.9
- w_query: float32 [2048, 2048], P('fs', 'tp'), may hold values from -0.125 to 0.125
- w_key: float32 [2048, 2048], P('fs', 'tp'), may hold values from -0.125 to 0.125
- w_value: float32 [2048, 2048], P('fs', 'tp'), may hold values from -0.125 to 0.125
- w_outgate: float32 [2048, 2048], P('fs', 'tp'), may hold values from -0.125 to 0.125
- scale_query: float32 [2048], P('tp'), may hold values from 0.5 to 2
- scale_key: float32 [2048], P('tp'), may hold values from 0.5 to 2
- scale_value: float32 [2048], P('tp'), may hold values from 0.5 to 2
- scale_outgate: float32 [2048], P('tp'), may hold values from 0.5 to 2
- ret_gain: float32 [2048], P('tp'), may hold values from 0.1 to 1.9
- decay_rate: float32 [8], P('tp'), may hold values from 0 to 2
- w_mix: float32 [2048, 2048], P('tp', 'fs'), may hold values from -0.125 to 0.125
- scale_mix: float32 [2048], P('tp'), may hold values from 0.5 to 2
- gain_two: float32 [2048], P('tp'), may hold values from 0.1 to 1.9
Outputs:
- layer_out: bfloat16 [6144, 2048], P('fs', 'tp')
All inputs are finite; a program needn't handle non-finite values.
Results may differ from a plain program's by a relative error of at most 0.022.
Values may be sent and summed in bfloat16 or wider, within the bound.
A program may use at most 128 MiB of HBM per device.

v0:
```python
import jax
import jax.numpy as jnp
from jax import lax
from jax.sharding import PartitionSpec as P

D = 2048
LEN = 256
BLK = 128
EPS = 1e-06
HEAD_EPS = 0.1


def rotate_pairs(values):
    paired = values.reshape(values.shape[:-1] + (values.shape[-1] // 2, 2))
    return jnp.stack((-paired[..., 1], paired[..., 0]), axis=-1).reshape(values.shape)


def retain(query_rows, key_rows, value_rows, decay_rate, length, block):
    highest = lax.Precision.HIGHEST
    total_rows = query_rows.shape[0]
    heads = decay_rate.shape[0]
    head_size = query_rows.shape[1] // heads
    sequences = total_rows // length
    nblocks = length // block

    def split_heads(values):
        return values.astype(jnp.float32).reshape(sequences, length, heads, head_size)

    freq = 1.0 / 10000.0 ** jnp.linspace(0.0, 1.0, head_size // 2, dtype=jnp.float32)
    freq = jnp.repeat(freq, 2)
    angles = jnp.arange(length, dtype=jnp.float32)[:, None] * freq[None, :]
    sines = jnp.sin(angles)[None, :, None, :]
    cosines = jnp.cos(angles)[None, :, None, :]
    queries = split_heads(query_rows)
    queries = queries * cosines + rotate_pairs(queries) * sines
    keys_all = split_heads(key_rows) * head_size ** (-0.5)
    keys_all = keys_all * cosines + rotate_pairs(keys_all) * sines
    values_all = split_heads(value_rows)
    log_decay = -decay_rate
    offsets = jnp.arange(block, dtype=jnp.float32)
    distance = offsets[:, None] - offsets[None, :]
    inside = jnp.where(
        distance >= 0, jnp.exp(log_decay[:, None, None] * jnp.maximum(distance, 0.0)), 0.0
    )
    query_decay = jnp.exp(log_decay[None, :] * (offsets[:, None] + 1.0))
    key_decay = jnp.exp(log_decay[None, :] * (block - 1.0 - offsets[:, None]))
    block_decay = jnp.exp(log_decay * block)

    def to_blocks(values):
        return jnp.moveaxis(values.reshape(sequences, nblocks, block, heads, head_size), 1, 0)

    def advance(carried, pieces):
        query_blk, key_blk, value_blk = pieces
        scores = jnp.einsum("snhd,smhd->shnm", query_blk, key_blk, precision=highest) * inside
        within = jnp.einsum("shnm,smhe->snhe", scores, value_blk, precision=highest)
        across = (
            jnp.einsum("snhd,shde->snhe", query_blk, carried, precision=highest)
            * query_decay[None, :, :, None]
        )
        weighted = key_blk * key_decay[None, :, :, None]
        carried = carried * block_decay[None, :, None, None] + jnp.einsum(
            "smhd,smhe->shde", weighted, value_blk, precision=highest
        )
        return (carried, within + across)

    initial = jnp.zeros((sequences, heads, head_size, head_size), jnp.float32)
    _, results = lax.scan(
        advance, initial, (to_blocks(queries), to_blocks(keys_all), to_blocks(values_all))
    )
    results = jnp.moveaxis(results, 0, 1).reshape(sequences, length, heads, head_size)
    results = results * lax.rsqrt(jnp.mean(results * results, axis=-1, keepdims=True) + HEAD_EPS)
    return results.reshape(total_rows, heads * head_size)


def normed_rows(hidden_in, norm_gain):
    widened = hidden_in.astype(jnp.float32)
    totals = lax.psum(jnp.sum(widened * widened, axis=1), "tp")
    scaled = widened * lax.rsqrt(totals / D + EPS)[:, None] * norm_gain
    return lax.all_gather(scaled.astype(jnp.bfloat16), "tp", axis=1, tiled=True)


def summed_share(partial_value):
    rounded = lax.optimization_barrier(partial_value.astype(jnp.bfloat16))
    return lax.psum_scatter(
        rounded.astype(jnp.float32).astype(jnp.bfloat16), "tp", scatter_dimension=1, tiled=True
    ).astype(jnp.float32)


def ffn_gathered(features, gate_low, up_low, down_low, scale_gate, scale_up):
    gate_add = jnp.dot(
        features,
        lax.all_gather(gate_low, "fs", axis=0, tiled=True),
        preferred_element_type=jnp.float32,
    )
    up_add = jnp.dot(
        features,
        lax.all_gather(up_low, "fs", axis=0, tiled=True),
        preferred_element_type=jnp.float32,
    )
    hidden = (jax.nn.silu(gate_add * scale_gate) * (up_add * scale_up)).astype(jnp.bfloat16)
    return jnp.dot(
        hidden,
        lax.all_gather(down_low, "fs", axis=1, tiled=True),
        preferred_element_type=jnp.float32,
    )


def per_device(
    tokens,
    gain_one,
    w_gate,
    w_up,
    w_down,
    scale_gate,
    scale_up,
    scale_down,
    gain_mix,
    w_query,
    w_key,
    w_value,
    w_outgate,
    scale_query,
    scale_key,
    scale_value,
    scale_outgate,
    ret_gain,
    decay_rate,
    w_mix,
    scale_mix,
    gain_two,
):
    norm_one, norm_mix, norm_two, down_cols, mix_cols = (
        gain_one,
        gain_mix,
        gain_two,
        scale_down,
        scale_mix,
    )
    gate_low = w_gate.astype(jnp.bfloat16)
    up_low = w_up.astype(jnp.bfloat16)
    down_low = w_down.astype(jnp.bfloat16)
    ffn_one = ffn_gathered(
        normed_rows(tokens, norm_one), gate_low, up_low, down_low, scale_gate, scale_up
    )
    first = (tokens.astype(jnp.float32) + 0.5 * summed_share(ffn_one) * down_cols).astype(
        jnp.bfloat16
    )
    features = normed_rows(first, norm_mix)
    pieces = (
        lax.all_gather(w_query.astype(jnp.bfloat16), "fs", axis=0, tiled=True),
        lax.all_gather(w_key.astype(jnp.bfloat16), "fs", axis=0, tiled=True),
        lax.all_gather(w_value.astype(jnp.bfloat16), "fs", axis=0, tiled=True),
        lax.all_gather(w_outgate.astype(jnp.bfloat16), "fs", axis=0, tiled=True),
    )
    query_pre, key_pre, value_pre, outgate_pre = tuple(
        (jnp.dot(features, piece, preferred_element_type=jnp.float32) for piece in pieces)
    )
    query_rows = (query_pre * scale_query).astype(jnp.bfloat16)
    key_rows = (key_pre * scale_key).astype(jnp.bfloat16)
    value_rows = (value_pre * scale_value).astype(jnp.bfloat16)
    outgate_rows = (outgate_pre * scale_outgate).astype(jnp.bfloat16)
    retained = retain(query_rows, key_rows, value_rows, decay_rate, LEN, BLK)
    mixed = (retained * ret_gain * jax.nn.silu(outgate_rows.astype(jnp.float32))).astype(
        jnp.bfloat16
    )
    mix_partial = jnp.dot(
        mixed,
        lax.all_gather(w_mix.astype(jnp.bfloat16), "fs", axis=1, tiled=True),
        preferred_element_type=jnp.float32,
    )
    second = (first.astype(jnp.float32) + summed_share(mix_partial) * mix_cols).astype(jnp.bfloat16)
    ffn_two = ffn_gathered(
        normed_rows(second, norm_two), gate_low, up_low, down_low, scale_gate, scale_up
    )
    result = (second.astype(jnp.float32) + 0.5 * summed_share(ffn_two) * down_cols).astype(
        jnp.bfloat16
    )
    return result


def solution(mesh):
    return jax.shard_map(
        per_device,
        mesh=mesh,
        in_specs=(
            P("fs", "tp"),
            P("tp"),
            P("fs", "tp"),
            P("fs", "tp"),
            P("tp", "fs"),
            P("tp"),
            P("tp"),
            P("tp"),
            P("tp"),
            P("fs", "tp"),
            P("fs", "tp"),
            P("fs", "tp"),
            P("fs", "tp"),
            P("tp"),
            P("tp"),
            P("tp"),
            P("tp"),
            P("tp"),
            P("tp"),
            P("tp", "fs"),
            P("tp"),
            P("tp"),
        ),
        out_specs=P("fs", "tp"),
        check_vma=False,
    )
```

profile of v0, /device:TPU:0, one launch (start us, length us, event | category | flops | bytes accessed | tf_op | source)
XLA Modules:
  0.0 710.8 jit_solution(11164169633599705700)
XLA Ops:
  8.0 8.4 %psum.21 = f32[768]{0:T(1024)S(1)} all-reduce(f32[768]{0:T(1024)S(1)} %fusion.31), channel_id=1, replica_groups=mesh['fs'=8,'tp'=4] {'tp'}, use_global_device_ids=true, to_apply=%region_1.0 | all-reduce | flops 768 | bytes 6144 | tf_op jit(solution)/shard_map/psum | solution.py:77
  21.7 26.0 %all-gather.12.cloned.1.call-done = bf16[768,2048]{1,0:T(8,128)(2,1)} async-done(((bf16[768,512]{1,0:T(8,128)(2,1)}), bf16[768,2048]{1,0:T(8,128)(2,1)}) %all-gather.12.cloned.1.call-update) | async-done | bytes 3145744 | tf_op jit(solution)/shard_map/all_gather | solution.py:79
  47.6 62.2 %all-gather.14.cloned.1.call-done = bf16[2048,768]{1,0:T(8,128)(2,1)} async-done(((bf16[256,768]{1,0:T(8,128)(2,1)}), bf16[2048,768]{1,0:T(8,128)(2,1)}) %all-gather.14.cloned.1.call-update) | async-done | bytes 3145744 | tf_op jit(solution)/shard_map/all_gather | solution.py:92
  109.9 6.8 fusion.60
  116.7 54.1 %all-gather.16.cloned.1.call-done = bf16[2048,768]{1,0:T(8,128)(2,1)} async-done(((bf16[256,768]{1,0:T(8,128)(2,1)}), bf16[2048,768]{1,0:T(8,128)(2,1)}) %all-gather.16.cloned.1.call-update) | async-done | bytes 3145744 | tf_op jit(solution)/shard_map/all_gather | solution.py:97
  170.8 63.2 %all-gather.18.cloned.1.call-done = bf16[768,2048]{1,0:T(8,128)(2,1)} async-done(((bf16[768,256]{1,0:T(8,128)(2,1)}), bf16[768,2048]{1,0:T(8,128)(2,1)}) %all-gather.18.cloned.1.call-update) | async-done | bytes 3145744 | tf_op jit(solution)/shard_map/all_gather | solution.py:103
  234.0 11.0 %convolution_convert_fusion.2 = bf16[768,2048]{1,0:T(8,128)(2,1)} fusion(bf16[768,2048]{1,0:T(8,128)(2,1)} %all-gather.18.cloned.1.call-done, f32[768,768]{1,0:T(8,128)} %fusion.60, bf16[768,2048]{1,0:T(8,128)(2,1)S(1)} %copy-done.28, bf16[2048,768]{1,0:T(8,128)(2,1)} %all-gather.16.cloned.1.call-done, f32[768]{0:T(1024)S(1)} %copy-done.29, ...), kind=kOutput, calls=%fused_computation.31 | convolution fusion | flops 4838129664 | bytes 14948352 | tf_op jit(solution)/shard_map/dot_general | solution.py:101
  246.9 34.2 %reduce-scatter.4.cloned.1.call-done = bf16[768,512]{1,0:T(8,128)(2,1)} async-done(((bf16[768,2048]{1,0:T(8,128)(2,1)}), bf16[768,512]{1,0:T(8,128)(2,1)}) %reduce-scatter.4.cloned.1.call-update) | async-done | bytes 786448 | tf_op jit(solution)/shard_map/reduce_scatter | solution.py:84
  282.7 5.9 psum.22
  295.2 8.3 %multiply_cosine_fusion = (f32[2,128,256]{1,0,2:T(2,128)S(1)}, f32[2,128,256]{1,0,2:T(2,128)}, f32[2,128,256]{1,0,2:T(2,128)}) fusion(f32[2,128]{1,0:T(2,128)S(1)} %multiply_add_fusion.1, f32[256]{0:T(256)S(1)} %mul.404), kind=kLoop, calls=%fused_computation.82 | loop fusion | flops 327680 | bytes 788480 | tf_op jit(solution)/shard_map/cos | solution.py:33
  303.5 28.7 %all-gather.26.cloned.1.call-done = bf16[2048,512]{1,0:T(8,128)(2,1)} async-done(((bf16[256,512]{1,0:T(8,128)(2,1)}), bf16[2048,512]{1,0:T(8,128)(2,1)}) %all-gather.26.cloned.1.call-update) | async-done | bytes 2097168 | tf_op jit(solution)/shard_map/all_gather | solution.py:150
  332.2 28.6 %all-gather.20.cloned.1.call-done = bf16[768,2048]{1,0:T(8,128)(2,1)} async-done(((bf16[768,512]{1,0:T(8,128)(2,1)}), bf16[768,2048]{1,0:T(8,128)(2,1)}) %all-gather.20.cloned.1.call-update) | async-done | bytes 3145744 | tf_op jit(solution)/shard_map/all_gather | solution.py:79
  369.1 43.0 %all-gather.22.cloned.1.call-done = bf16[2048,512]{1,0:T(8,128)(2,1)} async-done(((bf16[256,512]{1,0:T(8,128)(2,1)}), bf16[2048,512]{1,0:T(8,128)(2,1)}) %all-gather.22.cloned.1.call-update) | async-done | bytes 2097168 | tf_op jit(solution)/shard_map/all_gather | solution.py:151
  412.1 6.0 broadcast_multiply_fusion
  453.1 8.8 %all-gather.24.cloned.1.call-done = bf16[2048,512]{1,0:T(8,128)(2,1)} async-done(((bf16[256,512]{1,0:T(8,128)(2,1)}), bf16[2048,512]{1,0:T(8,128)(2,1)}) %all-gather.24.cloned.1.call-update) | async-done | bytes 2097168 | tf_op jit(solution)/shard_map/all_gather | solution.py:152
  477.7 32.1 %while.15 = (s32[]{:T(128)}, f32[3,2,256,256]{3,2,1,0:T(8,128)S(1)}, f32[2,3,128,2,256]{2,4,3,1,0:T(8,128)}, f32[2]{0:T(128)}, f32[2,3,128,2,256]{2,0,4,3,1:T(2,...) while((s32[]{:T(128)}, ...), condition=%wide.region_6.7_spmd.clone.clone.clone, body=%wide.region_5.6_spmd.clone.clone.clone.sunk | while | flops 1814266368 | bytes 24476680 | solution.py:67
  516.7 45.7 %all-gather.30.cloned.1.call-done = bf16[512,2048]{1,0:T(8,128)(2,1)} async-done(((bf16[512,256]{1,0:T(8,128)(2,1)}), bf16[512,2048]{1,0:T(8,128)(2,1)}) %all-gather.30.cloned.1.call-update) | async-done | bytes 2097168 | tf_op jit(solution)/shard_map/all_gather | solution.py:168
  562.5 8.9 %convolution_convert_fusion = bf16[768,2048]{1,0:T(8,128)(2,1)} fusion(bf16[512,2048]{1,0:T(8,128)(2,1)} %all-gather.30.cloned.1.call-done, f32[768,512]{1,0:T(8,128)} %bitcast.106, f32[768,512]{1,0:T(8,128)S(1)} %bitcast.105, bf16[768,2048]{1,0:T(8,128)(2,1)} %all-gather.20.cloned.1.call-done, bf16[2048,512]{1,0:T(8,128)(2,1)} %all-gather.28.cloned.1.call-done, ...), kind=kOutput, calls=%fused_computation.29 | convolution fusion | flops 3227123712 | bytes 13635584 | tf_op jit(solution)/shard_map/dot_general | solution.py:166
  571.5 36.0 %reduce-scatter.6.cloned.1.call-done = bf16[768,512]{1,0:T(8,128)(2,1)} async-done(((bf16[768,2048]{1,0:T(8,128)(2,1)}), bf16[768,512]{1,0:T(8,128)(2,1)}) %reduce-scatter.6.cloned.1.call-update) | async-done | bytes 786448 | tf_op jit(solution)/shard_map/reduce_scatter | solution.py:84
  609.0 5.8 psum.23
  616.0 29.2 %all-gather.32.cloned.1.call-done = bf16[768,2048]{1,0:T(8,128)(2,1)} async-done(((bf16[768,512]{1,0:T(8,128)(2,1)}), bf16[768,2048]{1,0:T(8,128)(2,1)}) %all-gather.32.cloned.1.call-update) | async-done | bytes 3145744 | tf_op jit(solution)/shard_map/all_gather | solution.py:79
  645.3 6.8 fusion.61
  652.1 11.8 %convolution_convert_fusion.1 = bf16[768,2048]{1,0:T(8,128)(2,1)} fusion(bf16[768,2048]{1,0:T(8,128)(2,1)} %all-gather.18.cloned.1.call-done, f32[768,768]{1,0:T(8,128)} %fusion.61, bf16[768,2048]{1,0:T(8,128)(2,1)} %all-gather.32.cloned.1.call-done, bf16[2048,768]{1,0:T(8,128)(2,1)} %all-gather.16.cloned.1.call-done, f32[768]{0:T(1024)S(1)} %copy-done.30, ...), kind=kOutput, calls=%fused_computation.30 | convolution fusion | flops 4838129664 | bytes 14948352 | tf_op jit(solution)/shard_map/dot_general | solution.py:101
  663.9 37.9 %reduce-scatter.8.cloned.1.call-done = bf16[768,512]{1,0:T(8,128)(2,1)} async-done(((bf16[768,2048]{1,0:T(8,128)(2,1)}), bf16[768,512]{1,0:T(8,128)(2,1)}) %reduce-scatter.8.cloned.1.call-update) | async-done | bytes 786448 | tf_op jit(solution)/shard_map/reduce_scatter | solution.py:84
  (197 shorter events, 119.3 us)
Async XLA Ops:
  6.5 41.1 %all-gather.12.cloned.1.call-start = ((), (), s32[]{:S(2)}) async-start(), calls=%async_computation.3 | async-start | bytes 3932160 | tf_op jit(solution)/shard_map/all_gather | solution.py:79
  18.7 91.2 %all-gather.14.cloned.1.call-start = ((), (), s32[]{:S(2)}) async-start(), calls=%async_computation.4 | async-start | bytes 3538944 | tf_op jit(solution)/shard_map/all_gather | solution.py:92
  19.5 151.2 %all-gather.16.cloned.1.call-start = ((), (), s32[]{:S(2)}) async-start(), calls=%async_computation.5 | async-start | bytes 3538944 | tf_op jit(solution)/shard_map/all_gather | solution.py:97
  20.7 213.3 %all-gather.18.cloned.1.call-start = ((), (), s32[]{:S(2)}) async-start(), calls=%async_computation.6 | async-start | bytes 3538944 | tf_op jit(solution)/shard_map/all_gather | solution.py:103
  21.6 212.4 %copy-start.29 = (f32[768]{0:T(1024)S(1)}, f32[768]{0:T(1024)}, u32[]{:S(2)}) copy-start(f32[768]{0:T(1024)} %param.30) | copy-start | bytes 9220
  21.6 212.4 %copy-start.31 = (f32[768]{0:T(1024)S(1)}, f32[768]{0:T(1024)}, u32[]{:S(2)}) copy-start(f32[768]{0:T(1024)} %param.29) | copy-start | bytes 9220
  21.6 259.5 %reduce-scatter.4.cloned.1.call-start = ((), (), s32[]{:S(2)}) async-start(), calls=%async_computation.7 | async-start | bytes 3932160 | tf_op jit(solution)/shard_map/reduce_scatter | solution.py:84
  47.6 186.4 %copy-start.28 = (bf16[768,2048]{1,0:T(8,128)(2,1)S(1)}, bf16[768,2048]{1,0:T(8,128)(2,1)}, u32[]{:S(2)}) copy-start(bf16[768,2048]{1,0:T(8,128)(2,1)} %all-gather.12.cloned.1.call-done) | copy-start | bytes 9437188
  245.1 43.5 %copy-start.24 = (f32[512]{0:T(512)S(1)}, f32[512]{0:T(512)}, u32[]{:S(2)}) copy-start(f32[512]{0:T(512)} %param.32) | copy-start | bytes 6148
  245.1 87.2 %all-gather.26.cloned.1.call-start = ((), (), s32[]{:S(2)}) async-start(), calls=%async_computation.11 | async-start | bytes 2359296 | tf_op jit(solution)/shard_map/all_gather | solution.py:150
  246.8 114.0 %all-gather.20.cloned.1.call-start = ((), (), s32[]{:S(2)}) async-start(), calls=%async_computation.8 | async-start | bytes 3932160 | tf_op jit(solution)/shard_map/all_gather | solution.py:79
  246.9 41.7 %copy-start.19 = (f32[512]{0:T(512)}, f32[512]{0:T(512)S(1)}, u32[]{:S(2)}) copy-start(f32[512]{0:T(512)S(1)} %broadcast_multiply_fusion.1) | copy-start | bytes 6148
  289.8 122.3 %all-gather.22.cloned.1.call-start = ((), (), s32[]{:S(2)}) async-start(), calls=%async_computation.9 | async-start | bytes 2359296 | tf_op jit(solution)/shard_map/all_gather | solution.py:151
  290.6 171.3 %all-gather.24.cloned.1.call-start = ((), (), s32[]{:S(2)}) async-start(), calls=%async_computation.10 | async-start | bytes 2359296 | tf_op jit(solution)/shard_map/all_gather | solution.py:152
  291.4 69.4 %copy-start.33 = (f32[512]{0:T(512)S(1)}, f32[512]{0:T(512)}, u32[]{:S(2)}) copy-start(f32[512]{0:T(512)} %param.37) | copy-start | bytes 6148
  291.5 225.3 %all-gather.28.cloned.1.call-start = ((), (), s32[]{:S(2)}) async-start(), calls=%async_computation.12 | async-start | bytes 2359296 | tf_op jit(solution)/shard_map/all_gather | solution.py:153
  292.3 270.2 %all-gather.30.cloned.1.call-start = ((), (), s32[]{:S(2)}) async-start(), calls=%async_computation.13 | async-start | bytes 2359296 | tf_op jit(solution)/shard_map/all_gather | solution.py:168
  293.1 314.4 %reduce-scatter.6.cloned.1.call-start = ((), (), s32[]{:S(2)}) async-start(), calls=%async_computation.14 | async-start | bytes 3932160 | tf_op jit(solution)/shard_map/reduce_scatter | solution.py:84
  366.9 45.2 %copy-start.34 = (f32[512]{0:T(512)S(1)}, f32[512]{0:T(512)}, u32[]{:S(2)}) copy-start(f32[512]{0:T(512)} %param.38) | copy-start | bytes 6148
  515.4 47.1 %copy-start.36 = (f32[512]{0:T(512)S(1)}, f32[512]{0:T(512)}, u32[]{:S(2)}) copy-start(f32[512]{0:T(512)} %param.40) | copy-start | bytes 6148
  515.4 47.0 %copy-start.37 = (f32[512]{0:T(512)S(1)}, f32[512]{0:T(512)}, u32[]{:S(2)}) copy-start(f32[512]{0:T(512)} %param.41) | copy-start | bytes 6148
  571.5 43.3 %copy-start.25 = (f32[512]{0:T(512)S(1)}, f32[512]{0:T(512)}, u32[]{:S(2)}) copy-start(f32[512]{0:T(512)} %param.45) | copy-start | bytes 6148
  571.5 73.8 %all-gather.32.cloned.1.call-start = ((), (), s32[]{:S(2)}) async-start(), calls=%async_computation.15 | async-start | bytes 3932160 | tf_op jit(solution)/shard_map/all_gather | solution.py:79
  616.0 85.8 %reduce-scatter.8.cloned.1.call-start = ((), (), s32[]{:S(2)}) async-start(), calls=%async_computation.16 | async-start | bytes 3932160 | tf_op jit(solution)/shard_map/reduce_scatter | solution.py:84
  (38 other events, 324.2 us)
Sparse Core Ops, SparseCore 0:
  18.8 28.8 all-gather.11
  49.8 60.0 all-gather.13
  112.1 58.6 all-gather.15
  172.7 61.3 all-gather.17
  245.2 35.8 reduce-scatter.3
  283.1 49.1 all-gather.25
  333.8 27.0 all-gather.19
  363.0 49.0 all-gather.21
  414.2 47.6 all-gather.23
  463.9 47.6 all-gather.27
  513.6 48.8 all-gather.29
  571.6 35.8 reduce-scatter.5
  616.1 29.1 all-gather.31
  664.1 37.7 reduce-scatter.7
where the time goes:
time: 718 us; the launch traced here: 711 us
  waiting for transfers between devices  498 us (69%)
  matrix products  81.8 us (11%)
  local copies, waits for them, and re-layouts  52.8 us (7%)
  other arithmetic  43.2 us (6%)
  blocking collectives  20 us (3%)
  between operations  13.9 us (2%)
    reduce_scatter x3, waiting for transfers between devices, summed_share(): lax.psum_scatter(rounded.astype(jnp.float32).astype(jnp.bfloat16), 'tp',...  108 us
    all_gather x3, waiting for transfers between devices, normed_rows(): return lax.all_gather(scaled.astype(jnp.bfloat16), 'tp', axis=1, tiled=True)  83.8 us
    all_gather x1, waiting for transfers between devices, ffn_gathered(): lax.all_gather(down_low, 'fs', axis=1, tiled=True)  63.2 us
    all_gather x1, waiting for transfers between devices, ffn_gathered(): lax.all_gather(gate_low, 'fs', axis=0, tiled=True)  62.2 us
    all_gather x1, waiting for transfers between devices, ffn_gathered(): lax.all_gather(up_low, 'fs', axis=0, tiled=True)  54.1 us
    all_gather x1, waiting for transfers between devices, per_device(): lax.all_gather(w_mix.astype(jnp.bfloat16), 'fs', axis=1, tiled=True)  45.7 us
    all_gather x1, waiting for transfers between devices, per_device(): lax.all_gather(w_key.astype(jnp.bfloat16), 'fs', axis=0, tiled=True)  43 us
    all_gather x1, waiting for transfers between devices, per_device(): lax.all_gather(w_query.astype(jnp.bfloat16), 'fs', axis=0, tiled=True)  28.7 us
  transfers between devices with their start and end apart: 14, of which 13 were waited for; matrix products, arithmetic and copies ran while one was open for 18% of the time, Pallas kernels for 0%

commit v1 on v0

--- a/solution.py
+++ b/solution.py
@@ -1,3 +1,4 @@
+import functools
 import jax
 import jax.numpy as jnp
 from jax import lax
@@ -8,6 +9,14 @@
 BLK = 128
 EPS = 1e-06
 HEAD_EPS = 0.1
+
+
+def mix_paths(shard_in, axis_id):
+    base_arr = jnp.concatenate(jax.lax.all_gather(shard_in, axis_name=axis_id), axis=1)
+    return base_arr
+
+
+load_stops_all_by_axis = functools.partial(mix_paths, axis_id="tp")
 
 
 def rotate_pairs(values):
@@ -76,7 +85,7 @@
     widened = hidden_in.astype(jnp.float32)
     totals = lax.psum(jnp.sum(widened * widened, axis=1), "tp")
     scaled = widened * lax.rsqrt(totals / D + EPS)[:, None] * norm_gain
-    return lax.all_gather(scaled.astype(jnp.bfloat16), "tp", axis=1, tiled=True)
+    return load_stops_all_by_axis(scaled.astype(jnp.bfloat16))
 
 
 def summed_share(partial_value):

time: 718 us -> 733 us (1.021)
  local copies, waits for them, and re-layouts: 52.8 us -> 79.7 us
  waiting for transfers between devices: 498 us -> 485 us
    all_gather x1, waiting for transfers between devices: 28.7 us -> 46.6 us  [per_device(): lax.all_gather(w_query.astype(jnp.bfloat16), 'fs', axis=0, tiled=True)]
    all_gather x3, waiting for transfers between devices: 83.8 us -> 70.2 us  [mix_paths(): jax.lax.all_gather(shard_in, axis_name=axis_id)]
    all_gather x0 -> x3, local copies, waits for them, and re-layouts: none -> 12.6 us  [mix_paths(): jax.lax.all_gather(shard_in, axis_name=axis_id)]
    reshape x4, local copies, waits for them, and re-layouts: 15.1 us -> 24.3 us  [split_heads(): values.astype(jnp.float32).reshape(sequences, length, heads, head_size)]
    all_gather x1, waiting for transfers between devices: 8.76 us -> 0.02 us  [per_device(): lax.all_gather(w_value.astype(jnp.bfloat16), 'fs', axis=0, tiled=True)]
  transfers between devices with their start and end apart: 14 -> 14, of which waited for: 13 -> 12; matrix products, arithmetic and copies ran while one was open for 18% -> 20% of each run, Pallas kernels for 0% -> 0%
where the time goes in v1:
time: 733 us; the launch traced here: 724 us
  waiting for transfers between devices  485 us (66%)
  matrix products  80.7 us (11%)
  local copies, waits for them, and re-layouts  79.7 us (11%)
  other arithmetic  43.4 us (6%)
  blocking collectives  20 us (3%)
  between operations  14 us (2%)
    reduce_scatter x3, waiting for transfers between devices, summed_share(): lax.psum_scatter(rounded.astype(jnp.float32).astype(jnp.bfloat16), 'tp',...  109 us
    all_gather x3, waiting for transfers between devices, mix_paths(): jax.lax.all_gather(shard_in, axis_name=axis_id)  70.2 us
    all_gather x1, waiting for transfers between devices, ffn_gathered(): lax.all_gather(down_low, 'fs', axis=1, tiled=True)  63.2 us
    all_gather x1, waiting for transfers between devices, ffn_gathered(): lax.all_gather(gate_low, 'fs', axis=0, tiled=True)  59 us
    all_gather x1, waiting for transfers between devices, ffn_gathered(): lax.all_gather(up_low, 'fs', axis=0, tiled=True)  54.9 us
    all_gather x1, waiting for transfers between devices, per_device(): lax.all_gather(w_query.astype(jnp.bfloat16), 'fs', axis=0, tiled=True)  46.6 us
    all_gather x1, waiting for transfers between devices, per_device(): lax.all_gather(w_key.astype(jnp.bfloat16), 'fs', axis=0, tiled=True)  41.6 us
    all_gather x1, waiting for transfers between devices, per_device(): lax.all_gather(w_mix.astype(jnp.bfloat16), 'fs', axis=1, tiled=True)  40.4 us
  transfers between devices with their start and end apart: 14, of which 12 were waited for; matrix products, arithmetic and copies ran while one was open for 20% of the time, Pallas kernels for 0%

profile of v1, /device:TPU:0, one launch (start us, length us, event | category | flops | bytes accessed | tf_op | source)
XLA Modules:
  0.0 724.0 jit_solution(8532640827104849418)
XLA Ops:
  8.0 8.4 %psum.21 = f32[768]{0:T(1024)S(1)} all-reduce(f32[768]{0:T(1024)S(1)} %fusion.31), channel_id=1, replica_groups=mesh['fs'=8,'tp'=4] {'tp'}, use_global_device_ids=true, to_apply=%region_1.0 | all-reduce | flops 768 | bytes 6144 | tf_op jit(solution)/shard_map/psum | solution.py:86
  21.6 26.0 %all-gather.31.cloned.1.call-done = bf16[3072,512]{1,0:T(8,128)(2,1)} async-done(((bf16[768,512]{1,0:T(8,128)(2,1)}), bf16[3072,512]{1,0:T(8,128)(2,1)}) %all-gather.31.cloned.1.call-update) | async-done | bytes 3145744 | tf_op jit(solution)/shard_map/all_gather | solution.py:15
  50.8 59.0 %all-gather.15.cloned.1.call-done = bf16[2048,768]{1,0:T(8,128)(2,1)} async-done(((bf16[256,768]{1,0:T(8,128)(2,1)}), bf16[2048,768]{1,0:T(8,128)(2,1)}) %all-gather.15.cloned.1.call-update) | async-done | bytes 3145744 | tf_op jit(solution)/shard_map/all_gather | solution.py:101
  109.9 6.0 fusion.60
  115.9 54.9 %all-gather.17.cloned.1.call-done = bf16[2048,768]{1,0:T(8,128)(2,1)} async-done(((bf16[256,768]{1,0:T(8,128)(2,1)}), bf16[2048,768]{1,0:T(8,128)(2,1)}) %all-gather.17.cloned.1.call-update) | async-done | bytes 3145744 | tf_op jit(solution)/shard_map/all_gather | solution.py:106
  170.8 63.2 %all-gather.19.cloned.1.call-done = bf16[768,2048]{1,0:T(8,128)(2,1)} async-done(((bf16[768,256]{1,0:T(8,128)(2,1)}), bf16[768,2048]{1,0:T(8,128)(2,1)}) %all-gather.19.cloned.1.call-update) | async-done | bytes 3145744 | tf_op jit(solution)/shard_map/all_gather | solution.py:112
  234.0 11.4 %convolution_convert_fusion.2 = bf16[768,2048]{1,0:T(8,128)(2,1)} fusion(bf16[768,2048]{1,0:T(8,128)(2,1)} %all-gather.19.cloned.1.call-done, f32[768,768]{1,0:T(8,128)} %fusion.60, bf16[768,2048]{0,1:T(8,128)(2,1)S(1)} %bitcast.124, bf16[2048,768]{1,0:T(8,128)(2,1)} %all-gather.17.cloned.1.call-done, f32[768]{0:T(1024)S(1)} %copy-done.32, ...), kind=kOutput, calls=%fused_computation.31 | convolution fusion | flops 4838129664 | bytes 14948352 | tf_op jit(solution)/shard_map/dot_general | solution.py:110
  246.1 35.4 %reduce-scatter.4.cloned.1.call-done = bf16[768,512]{1,0:T(8,128)(2,1)} async-done(((bf16[768,2048]{1,0:T(8,128)(2,1)}), bf16[768,512]{1,0:T(8,128)(2,1)}) %reduce-scatter.4.cloned.1.call-update) | async-done | bytes 786448 | tf_op jit(solution)/shard_map/reduce_scatter | solution.py:93
  283.0 5.9 psum.22
  295.9 8.6 %multiply_cosine_fusion = (f32[2,128,256]{1,0,2:T(2,128)S(1)}, f32[2,128,256]{1,0,2:T(2,128)}, f32[2,128,256]{1,0,2:T(2,128)}) fusion(f32[2,128]{1,0:T(2,128)S(1)} %multiply_add_fusion.1, f32[256]{0:T(256)S(1)} %mul.404), kind=kLoop, calls=%fused_computation.82 | loop fusion | flops 327680 | bytes 788480 | tf_op jit(solution)/shard_map/cos | solution.py:42
  304.5 14.9 %all-gather.33.cloned.1.call-done = bf16[3072,512]{1,0:T(8,128)(2,1)} async-done(((bf16[768,512]{1,0:T(8,128)(2,1)}), bf16[3072,512]{1,0:T(8,128)(2,1)}) %all-gather.33.cloned.1.call-update) | async-done | bytes 3145744 | tf_op jit(solution)/shard_map/all_gather | solution.py:15
  324.1 46.6 %all-gather.25.cloned.1.call-done = bf16[2048,512]{1,0:T(8,128)(2,1)} async-done(((bf16[256,512]{1,0:T(8,128)(2,1)}), bf16[2048,512]{1,0:T(8,128)(2,1)}) %all-gather.25.cloned.1.call-update) | async-done | bytes 2097168 | tf_op jit(solution)/shard_map/all_gather | solution.py:159
  378.9 41.6 %all-gather.21.cloned.1.call-done = bf16[2048,512]{1,0:T(8,128)(2,1)} async-done(((bf16[256,512]{1,0:T(8,128)(2,1)}), bf16[2048,512]{1,0:T(8,128)(2,1)}) %all-gather.21.cloned.1.call-update) | async-done | bytes 2097168 | tf_op jit(solution)/shard_map/all_gather | solution.py:160
  420.5 5.5 broadcast_multiply_fusion
  457.6 14.3 %copy.70 = f32[3,2,128,2,256]{2,1,4,3,0:T(2,128)} copy(f32[3,2,128,2,256]{4,3,2,1,0:T(2,128)} %reshape.177) | data formatting | bytes 3145728 | tf_op jit(solution)/shard_map/reshape | solution.py:36
  487.8 31.9 %while.15 = (s32[]{:T(128)}, f32[3,2,256,256]{3,2,1,0:T(8,128)S(1)}, f32[2,3,128,2,256]{2,4,3,1,0:T(8,128)}, f32[2]{0:T(128)}, f32[2,3,128,2,256]{2,0,4,3,1:T(2,...) while((s32[]{:T(128)}, ...), condition=%wide.region_6.7_spmd.clone.clone.clone, body=%wide.region_5.6_spmd.clone.clone.clone.sunk | while | flops 1814266368 | bytes 24476680 | solution.py:76
  530.5 40.4 %all-gather.29.cloned.1.call-done = bf16[512,2048]{1,0:T(8,128)(2,1)} async-done(((bf16[512,256]{1,0:T(8,128)(2,1)}), bf16[512,2048]{1,0:T(8,128)(2,1)}) %all-gather.29.cloned.1.call-update) | async-done | bytes 2097168 | tf_op jit(solution)/shard_map/all_gather | solution.py:177
  570.8 8.6 %convolution_convert_fusion = bf16[768,2048]{1,0:T(8,128)(2,1)} fusion(bf16[512,2048]{1,0:T(8,128)(2,1)} %all-gather.29.cloned.1.call-done, f32[768,512]{1,0:T(8,128)} %bitcast.129, f32[768,512]{1,0:T(8,128)} %bitcast.128, bf16[768,2048]{0,1:T(8,128)(2,1)S(1)} %bitcast.118, bf16[2048,512]{1,0:T(8,128)(2,1)} %all-gather.27.cloned.1.call-done, ...), kind=kOutput, calls=%fused_computation.29 | convolution fusion | flops 3227123712 | bytes 13635584 | tf_op jit(solution)/shard_map/dot_general | solution.py:175
  579.5 36.0 %reduce-scatter.6.cloned.1.call-done = bf16[768,512]{1,0:T(8,128)(2,1)} async-done(((bf16[768,2048]{1,0:T(8,128)(2,1)}), bf16[768,512]{1,0:T(8,128)(2,1)}) %reduce-scatter.6.cloned.1.call-update) | async-done | bytes 786448 | tf_op jit(solution)/shard_map/reduce_scatter | solution.py:93
  617.0 5.8 psum.23
  624.0 29.2 %all-gather.35.cloned.1.call-done = bf16[3072,512]{1,0:T(8,128)(2,1)} async-done(((bf16[768,512]{1,0:T(8,128)(2,1)}), bf16[3072,512]{1,0:T(8,128)(2,1)}) %all-gather.35.cloned.1.call-update) | async-done | bytes 3145744 | tf_op jit(solution)/shard_map/all_gather | solution.py:15
  657.9 6.9 fusion.61
  664.9 12.1 %convolution_convert_fusion.1 = bf16[768,2048]{1,0:T(8,128)(2,1)} fusion(bf16[768,2048]{1,0:T(8,128)(2,1)} %all-gather.19.cloned.1.call-done, f32[768,768]{1,0:T(8,128)} %fusion.61, bf16[768,2048]{0,1:T(8,128)(2,1)} %bitcast.127, bf16[2048,768]{1,0:T(8,128)(2,1)} %all-gather.17.cloned.1.call-done, f32[768]{0:T(1024)S(1)} %copy-done.33, f32[768]{0:T(1024)S(1)} %copy-done.35), kind=kOutput, calls=%fused_computation.30 | convolution fusion | flops 4838129664 | bytes 14948352 | tf_op jit(solution)/shard_map/dot_general | solution.py:110
  677.0 37.9 %reduce-scatter.8.cloned.1.call-done = bf16[768,512]{1,0:T(8,128)(2,1)} async-done(((bf16[768,2048]{1,0:T(8,128)(2,1)}), bf16[768,512]{1,0:T(8,128)(2,1)}) %reduce-scatter.8.cloned.1.call-update) | async-done | bytes 786448 | tf_op jit(solution)/shard_map/reduce_scatter | solution.py:93
  (200 shorter events, 131.2 us)
Async XLA Ops:
  6.5 41.1 %all-gather.31.cloned.1.call-start = ((), (), s32[]{:S(2)}) async-start(), calls=%async_computation.14 | async-start | bytes 3932160 | tf_op jit(solution)/shard_map/all_gather | solution.py:15
  18.7 91.2 %all-gather.15.cloned.1.call-start = ((), (), s32[]{:S(2)}) async-start(), calls=%async_computation.3 | async-start | bytes 3538944 | tf_op jit(solution)/shard_map/all_gather | solution.py:101
  19.5 151.2 %all-gather.17.cloned.1.call-start = ((), (), s32[]{:S(2)}) async-start(), calls=%async_computation.4 | async-start | bytes 3538944 | tf_op jit(solution)/shard_map/all_gather | solution.py:106
  20.7 213.3 %all-gather.19.cloned.1.call-start = ((), (), s32[]{:S(2)}) async-start(), calls=%async_computation.5 | async-start | bytes 3538944 | tf_op jit(solution)/shard_map/all_gather | solution.py:112
  21.6 259.9 %reduce-scatter.4.cloned.1.call-start = ((), (), s32[]{:S(2)}) async-start(), calls=%async_computation.6 | async-start | bytes 3932160 | tf_op jit(solution)/shard_map/reduce_scatter | solution.py:93
  109.9 124.2 %copy-start.32 = (f32[768]{0:T(1024)S(1)}, f32[768]{0:T(1024)}, u32[]{:S(2)}) copy-start(f32[768]{0:T(1024)} %param.30) | copy-start | bytes 9220
  109.9 124.2 %copy-start.34 = (f32[768]{0:T(1024)S(1)}, f32[768]{0:T(1024)}, u32[]{:S(2)}) copy-start(f32[768]{0:T(1024)} %param.29) | copy-start | bytes 9220
  245.4 43.5 %copy-start.28 = (f32[512]{0:T(512)S(1)}, f32[512]{0:T(512)}, u32[]{:S(2)}) copy-start(f32[512]{0:T(512)} %param.32) | copy-start | bytes 6148
  245.4 74.0 %all-gather.33.cloned.1.call-start = ((), (), s32[]{:S(2)}) async-start(), calls=%async_computation.15 | async-start | bytes 3932160 | tf_op jit(solution)/shard_map/all_gather | solution.py:15
  246.1 42.9 %copy-start.23 = (f32[512]{0:T(512)}, f32[512]{0:T(512)S(1)}, u32[]{:S(2)}) copy-start(f32[512]{0:T(512)S(1)} %broadcast_multiply_fusion.1) | copy-start | bytes 6148
  290.1 80.5 %all-gather.25.cloned.1.call-start = ((), (), s32[]{:S(2)}) async-start(), calls=%async_computation.9 | async-start | bytes 2359296 | tf_op jit(solution)/shard_map/all_gather | solution.py:159
  291.0 129.5 %all-gather.21.cloned.1.call-start = ((), (), s32[]{:S(2)}) async-start(), calls=%async_computation.7 | async-start | bytes 2359296 | tf_op jit(solution)/shard_map/all_gather | solution.py:160
  291.8 180.2 %all-gather.23.cloned.1.call-start = ((), (), s32[]{:S(2)}) async-start(), calls=%async_computation.8 | async-start | bytes 2359296 | tf_op jit(solution)/shard_map/all_gather | solution.py:161
  292.7 237.8 %all-gather.27.cloned.1.call-start = ((), (), s32[]{:S(2)}) async-start(), calls=%async_computation.10 | async-start | bytes 2359296 | tf_op jit(solution)/shard_map/all_gather | solution.py:162
  293.5 277.3 %all-gather.29.cloned.1.call-start = ((), (), s32[]{:S(2)}) async-start(), calls=%async_computation.11 | async-start | bytes 2359296 | tf_op jit(solution)/shard_map/all_gather | solution.py:177
  294.3 321.2 %reduce-scatter.6.cloned.1.call-start = ((), (), s32[]{:S(2)}) async-start(), calls=%async_computation.12 | async-start | bytes 3932160 | tf_op jit(solution)/shard_map/reduce_scatter | solution.py:93
  319.4 51.3 %copy-start.18 = (f32[512]{0:T(512)S(1)}, f32[512]{0:T(512)}, u32[]{:S(2)}) copy-start(f32[512]{0:T(512)} %param.37) | copy-start | bytes 6148
  376.7 43.7 %copy-start.19 = (f32[512]{0:T(512)S(1)}, f32[512]{0:T(512)}, u32[]{:S(2)}) copy-start(f32[512]{0:T(512)} %param.38) | copy-start | bytes 6148
  523.7 47.2 %copy-start.37 = (f32[512]{0:T(512)S(1)}, f32[512]{0:T(512)}, u32[]{:S(2)}) copy-start(f32[512]{0:T(512)} %param.41) | copy-start | bytes 6148
  527.6 43.3 %copy-start.1 = (bf16[4,768,512]{1,2,0:T(8,128)(2,1)S(1)}, bf16[4,768,512]{1,2,0:T(8,128)(2,1)}, u32[]{:S(2)}) copy-start(bf16[4,768,512]{1,2,0:T(8,128)(2,1)} %copy.65) | copy-start | bytes 9437188
  527.6 43.3 %copy-start.36 = (f32[512]{0:T(512)S(1)}, f32[512]{0:T(512)}, u32[]{:S(2)}) copy-start(f32[512]{0:T(512)} %param.40) | copy-start | bytes 6148
  579.4 43.4 %copy-start.29 = (f32[512]{0:T(512)S(1)}, f32[512]{0:T(512)}, u32[]{:S(2)}) copy-start(f32[512]{0:T(512)} %param.45) | copy-start | bytes 6148
  579.4 73.8 %all-gather.35.cloned.1.call-start = ((), (), s32[]{:S(2)}) async-start(), calls=%async_computation.16 | async-start | bytes 3932160 | tf_op jit(solution)/shard_map/all_gather | solution.py:15
  624.0 90.9 %reduce-scatter.8.cloned.1.call-start = ((), (), s32[]{:S(2)}) async-start(), calls=%async_computation.13 | async-start | bytes 3932160 | tf_op jit(solution)/shard_map/reduce_scatter | solution.py:93
  (38 other events, 266.1 us)
Sparse Core Ops, SparseCore 0:
  18.8 28.8 all-gather.30
  49.8 60.0 all-gather.14
  112.1 58.6 all-gather.16
  172.7 61.3 all-gather.18
  245.5 35.8 reduce-scatter.3
  290.2 29.1 all-gather.32
  321.5 49.0 all-gather.24
  372.8 47.6 all-gather.20
  422.6 47.5 all-gather.22
  472.2 47.6 all-gather.26
  521.9 48.8 all-gather.28
  579.5 35.8 reduce-scatter.5
  624.1 29.1 all-gather.34
  677.1 37.7 reduce-scatter.7
